TPU v7x, 32 devices: a whole 2x2x4 slice. The times are simulated.
32 devices in a mesh: sp: 8 (over z, x), tp: 4 (over y, core).
Axes of the slice: x: 2, y: 2, z: 4, core: 2. Of those that a mesh axis runs over, the one named last changes fastest.
Arguments:
- residual_in: bfloat16 [1536, 2048], P('sp', 'tp'), may hold values from -6 to 6
- query_rows: bfloat16 [1536, 1024], P('sp', 'tp'), may hold values from -8 to 8
- key_rows: bfloat16 [1536, 1024], P('sp', 'tp'), may hold values from -8 to 8
- value_rows: bfloat16 [1536, 1024], P('sp', 'tp'), may hold values from -6 to 6
- map_weight: float32 [16], P('tp'), may hold values from 0.3 to 0.8
- head_gain: float32 [64], replicated, may hold values from 0.1 to 1.9
- out_proj: bfloat16 [1024, 2048], P(None, 'tp'), may hold values from -0.1875 to 0.1875
- norm_gain: float32 [2048], replicated, may hold values from 0.1 to 1.9
- route_ids: int32 [1536, 2], P('sp'), may hold values from 0 to 7, all different within a row; in each aligned block of 192 rows (0 to 191, 192 to 383, ...) at most 60 rows name the same one
- route_weights: float32 [1536, 2], P('sp'), may hold values from 0.2 to 1.2
- expert_gate: bfloat16 [8, 1024, 2048], P('sp', 'tp'), may hold values from -0.125 to 0.125
- expert_up: bfloat16 [8, 1024, 2048], P('sp', 'tp'), may hold values from -0.125 to 0.125
- expert_down: bfloat16 [8, 1024, 2048], P('sp', None, 'tp'), may hold values from -0.1875 to 0.1875
- shared_gate: bfloat16 [1024, 2048], P('tp'), may hold values from -0.125 to 0.125
- shared_up: bfloat16 [1024, 2048], P('tp'), may hold values from -0.125 to 0.125
- shared_down: bfloat16 [1024, 2048], P(None, 'tp'), may hold values from -0.1875 to 0.1875
Outputs:
- mixed_out: bfloat16 [1536, 2048], P('sp', 'tp')
Inputs may be any that keep to these rules, and one draw needn't show every extreme that they name: `route_ids`: each row names 2 different experts. Among the rows held by one index of sp no expert is named more than 60 times, and in every draw some expert is named exactly 60 times by the rows of some index of sp.
All inputs are finite; a program needn't handle non-finite values.
Results may differ from a plain program's by a relative error of at most 0.0095.
Values may be sent and summed in bfloat16 or wider, within the bound.
No kernel may reach another device: no remote copies, remote signals or barrier semaphores. Data moves between devices by JAX's collectives and lax.ppermute only.
A program may use at most 64 MiB of HBM per device.

v0:
```python
import jax
import jax.numpy as jnp
from jax import lax
from jax.sharding import PartitionSpec as P

epsilon = 1e-06
masked_score = -1e30


def rms_scale(values, gain_vec):
    squares = jnp.mean(values * values, axis=-1, keepdims=True)
    return values * lax.rsqrt(squares + epsilon) * gain_vec


def block_slots(route_block, experts_all, capacity):
    flat_ids = route_block.reshape(-1)
    one_hot = (flat_ids[:, None] == jnp.arange(experts_all, dtype=jnp.int32)[None, :]).astype(
        jnp.int32
    )
    earlier = jnp.cumsum(one_hot, axis=0) - one_hot
    position = jnp.sum(earlier * one_hot, axis=1)
    return (flat_ids * capacity + position).reshape(route_block.shape)


def body(
    residual_in,
    query_rows,
    key_rows,
    value_rows,
    map_weight,
    head_gain,
    out_proj,
    norm_gain,
    route_ids,
    route_weights,
    expert_gate,
    expert_up,
    expert_down,
    shared_gate,
    shared_up,
    shared_down,
):
    seq_dev = residual_in.shape[0]
    col_dev = residual_in.shape[1]
    heads_here = map_weight.shape[0]
    head_dim = head_gain.shape[0]
    half_dim = head_dim // 2
    topk_count = route_ids.shape[1]
    exp_here = expert_gate.shape[0]
    experts_all = exp_here * lax.axis_size("sp")
    capacity = 5 * seq_dev * topk_count // (4 * experts_all)
    score_scale = half_dim ** (-0.5)
    query_pos = lax.axis_index("sp") * seq_dev + jnp.arange(seq_dev, dtype=jnp.int32)
    query_heads = query_rows.reshape(seq_dev, heads_here, 2, half_dim)
    key_piece = lax.all_gather(key_rows, "sp", axis=0, tiled=True)
    value_piece = lax.all_gather(value_rows, "sp", axis=0, tiled=True)
    piece_len = key_piece.shape[0]
    key_heads = key_piece.reshape(piece_len, heads_here, 2, half_dim)
    value_heads = value_piece.reshape(piece_len, heads_here, head_dim)
    scores = (
        jnp.einsum("qhmd,khmd->mhqk", query_heads, key_heads, preferred_element_type=jnp.float32)
        * score_scale
    )
    key_pos = jnp.arange(piece_len, dtype=jnp.int32)
    visible = key_pos[None, :] <= query_pos[:, None]
    scores = jnp.where(visible, scores, masked_score)
    run_max = jnp.full((2, heads_here, seq_dev), masked_score, jnp.float32)
    new_max = jnp.maximum(run_max, jnp.max(scores, axis=-1))
    expo = jnp.where(visible, jnp.exp(scores - new_max[..., None]), 0.0)
    new_sum = jnp.sum(expo, axis=-1)
    product = jnp.einsum(
        "mhqk,khd->mhqd", expo.astype(jnp.bfloat16), value_heads, preferred_element_type=jnp.float32
    )
    summed = product / new_sum[..., None]
    diff_out = summed[0] - map_weight[:, None, None] * summed[1]
    head_out = rms_scale(diff_out, head_gain).astype(jnp.bfloat16)
    head_out = jnp.transpose(head_out, (1, 0, 2)).reshape(seq_dev, heads_here * head_dim)
    attn = jnp.dot(
        lax.all_gather(head_out, "tp", axis=1, tiled=True),
        out_proj,
        preferred_element_type=jnp.float32,
    )
    hidden_state = (residual_in.astype(jnp.float32) + attn).astype(jnp.bfloat16)
    full_rows = lax.all_gather(hidden_state, "tp", axis=1, tiled=True)
    normed = rms_scale(full_rows.astype(jnp.float32), norm_gain).astype(jnp.bfloat16)
    shared_gate_part = jnp.einsum(
        "rd,fd->rf", normed, shared_gate, preferred_element_type=jnp.float32
    )
    shared_up_part = jnp.einsum("rd,fd->rf", normed, shared_up, preferred_element_type=jnp.float32)
    shared_hidden = (jax.nn.silu(shared_gate_part) * shared_up_part).astype(jnp.bfloat16)
    slot_ids = block_slots(route_ids, experts_all, capacity)
    token_of = jnp.repeat(jnp.arange(seq_dev, dtype=jnp.int32), topk_count)
    slot_token = (
        jnp.full((experts_all * capacity,), seq_dev, jnp.int32)
        .at[slot_ids.reshape(-1)]
        .set(token_of)
    )
    own_cols = lax.dynamic_slice_in_dim(normed, lax.axis_index("tp") * col_dev, col_dev, 1)
    padded = jnp.concatenate([own_cols, jnp.zeros((1, col_dev), jnp.bfloat16)], axis=0)
    outgoing = jnp.take(padded, slot_token, axis=0).reshape(experts_all, capacity, col_dev)
    arrived = lax.all_to_all(outgoing, "sp", split_axis=0, concat_axis=1, tiled=True)
    arrived_rows = arrived.shape[1]
    pieces = lax.all_gather(arrived, "tp", axis=2, tiled=True)
    gate_add = jnp.einsum("erd,efd->erf", pieces, expert_gate, preferred_element_type=jnp.float32)
    up_add = jnp.einsum("erd,efd->erf", pieces, expert_up, preferred_element_type=jnp.float32)
    expert_hidden = (jax.nn.silu(gate_add) * up_add).astype(jnp.bfloat16)
    expert_flat = expert_hidden.reshape(exp_here * arrived_rows, expert_hidden.shape[2])
    pieces = (
        lax.all_gather(shared_hidden, "tp", axis=1, tiled=True),
        lax.all_gather(expert_flat, "tp", axis=1, tiled=True),
    )
    piece_width = pieces[0].shape[1]
    routed_piece = pieces[1].reshape(exp_here, arrived_rows, piece_width)
    shared_add = jnp.dot(pieces[0], shared_down, preferred_element_type=jnp.float32)
    expert_add = jnp.einsum(
        "erf,efd->erd", routed_piece, expert_down, preferred_element_type=jnp.float32
    )
    returned_rows = lax.all_to_all(
        expert_add.astype(jnp.bfloat16), "sp", split_axis=1, concat_axis=0, tiled=True
    )
    returned_flat = returned_rows.reshape(experts_all * capacity, col_dev)
    picked = (
        jnp.take(returned_flat, slot_ids.reshape(-1), axis=0)
        .reshape(seq_dev, topk_count, col_dev)
        .astype(jnp.float32)
    )
    routed = jnp.sum(picked * route_weights[:, :, None], axis=1)
    return (hidden_state.astype(jnp.float32) + shared_add + routed).astype(jnp.bfloat16)


def solution(mesh):
    in_specs = (
        P("sp", "tp"),
        P("sp", "tp"),
        P("sp", "tp"),
        P("sp", "tp"),
        P("tp"),
        P(),
        P(None, "tp"),
        P(),
        P("sp", None),
        P("sp", None),
        P("sp", "tp", None),
        P("sp", "tp", None),
        P("sp", None, "tp"),
        P("tp", None),
        P("tp", None),
        P(None, "tp"),
    )
    out_specs = P("sp", "tp")
    return jax.shard_map(body, mesh=mesh, in_specs=in_specs, out_specs=out_specs, check_vma=False)
```

profile of v0, /device:TPU:0, one launch (start us, length us, event | category | flops | bytes accessed | tf_op | source)
XLA Modules:
  0.0 206.6 jit_solution(2744693201549045714)
XLA Ops:
  6.5 0.9 copy.68
  7.7 0.7 broadcast_multiply_fusion
  8.4 0.8 reduce-window.6
  10.1 2.9 %scatter_custom_fusion = s32[480]{0:T(512)S(1)} fusion(s32[384]{0:T(512)S(1)} %fusion.40, s32[384]{0:T(512)S(1)} %reshape.188, s32[]{:T(128)} %constant.26.clone.1), kind=kCustom, calls=%fused_computation.66 | custom fusion | bytes 1924 | tf_op jit(solution)/shard_map/scatter | solution.py:96
  13.3 34.1 %all_gather.21 = bf16[1536,256]{1,0:T(8,128)(2,1)S(1)} all-gather(bf16[192,256]{1,0:T(8,128)(2,1)} %param.18), channel_id=1, replica_groups=mesh['sp'=8,'tp'=4] {'sp'}, dimensions={0}, use_global_device_ids=true | all-gather | bytes 884736 | tf_op jit(solution)/shard_map/all_gather | solution.py:55
  47.6 1.0 copy.60
  48.6 1.9 fusion
  50.5 4.4 %fusion.1 = (f32[2,4,192]{2,1,0:T(4,128)S(1)}, bf16[2,4,192,1536]{3,2,1,0:T(8,128)(2,1)}) fusion(f32[2,4,192,1536]{3,2,1,0:T(8,128)S(1)} %get-tuple-element.8, f32[2,4,192]{2,1,0:T(4,128)S(1)} %broadcast_maximum_fusion, pred[192,1536]{1,0:T(8,128)(4,1)S(1)} %iota_compare_fusion), kind=kLoop, calls=%fused_computation.6 | loop fusion | flops 14154240 | bytes 14462976 | tf_op jit(solution)/shard_map/reduce_sum | solution.py:70
  55.0 32.1 %all_gather.22 = bf16[1536,256]{1,0:T(8,128)(2,1)S(1)} all-gather(bf16[192,256]{1,0:T(8,128)(2,1)S(1)} %copy-done.2), channel_id=1, replica_groups=mesh['sp'=8,'tp'=4] {'sp'}, dimensions={0}, use_global_device_ids=true | all-gather | bytes 884736 | tf_op jit(solution)/shard_map/all_gather | solution.py:56
  87.4 4.0 %fusion.29 = f32[2,4,192,64]{2,3,0,1:T(8,128)S(1)} fusion(bf16[1536,4,64,1]{0,2,3,1:T(8,128)(2,1)S(1)} %bitcast.84, bf16[2,4,192,1536]{3,2,1,0:T(8,128)(2,1)} %get-tuple-element.6, f32[2,4,192]{2,0,1:T(2,128)S(1)} %copy.66), kind=kOutput, calls=%fused_computation.35 | convolution fusion | flops 302088192 | bytes 5904384 | tf_op jit(solution)/shard_map/mhqk,khd->mhqd/dot_general | solution.py:71
  91.7 7.2 %all_gather.23 = bf16[192,1024]{0,1:T(8,128)(2,1)S(1)} all-gather(bf16[192,256]{0,1:T(8,128)(2,1)S(1)} %bitcast.85), channel_id=1, replica_groups=mesh['sp'=8,'tp'=4] {'tp'}, dimensions={1}, use_global_device_ids=true | all-gather | bytes 491520 | tf_op jit(solution)/shard_map/all_gather | solution.py:79
  98.9 1.1 fusion.23
  100.0 8.9 %all_gather.24 = bf16[192,2048]{1,0:T(8,128)(2,1)S(1)} all-gather(bf16[192,512]{1,0:T(8,128)(2,1)} %fusion.23), channel_id=1, replica_groups=mesh['sp'=8,'tp'=4] {'tp'}, dimensions={1}, use_global_device_ids=true | all-gather | bytes 983040 | tf_op jit(solution)/shard_map/all_gather | solution.py:84
  109.5 2.1 %gather_fusion = bf16[480,512]{1,0:T(8,128)(2,1)S(1)} fusion(bf16[193,512]{1,0:T(8,128)(2,1)S(1)} %concatenate.3, s32[1024]{0:T(1024)S(1)} %pad_clamp_fusion.1), kind=kCustom, calls=%fused_computation | custom fusion | bytes 984960 | tf_op jit(solution)/shard_map/jit(_take)/gather | solution.py:100
  112.0 20.3 %all_to_all.21 = bf16[8,60,512]{2,1,0:T(8,128)(2,1)S(1)} all-to-all(bf16[8,60,512]{2,1,0:T(8,128)(2,1)S(1)} %broadcast_select_fusion.1), channel_id=1, replica_groups=mesh['sp'=8,'tp'=4] {'sp'}, dimensions={0} | all-to-all | bytes 983040 | tf_op jit(solution)/shard_map/all_to_all | solution.py:101
  132.3 0.9 all_to_all.7
  133.4 20.1 %all-gather.2.cloned.1.call-done = bf16[1,480,2048]{2,1,0:T(8,128)(2,1)} async-done(((bf16[1,480,512]{2,1,0:T(8,128)(2,1)}), bf16[1,480,2048]{2,1,0:T(8,128)(2,1)}) %all-gather.2.cloned.1.call-update) | async-done | bytes 1966096 | tf_op jit(solution)/shard_map/all_gather | solution.py:103
  153.6 2.7 %fusion.7 = f32[480,256]{1,0:T(8,128)S(1)} fusion(bf16[1,480,2048]{2,1,0:T(8,128)(2,1)} %all-gather.2.cloned.1.call-done, bf16[1,256,2048]{2,1,0:T(8,128)(2,1)} %param.26), kind=kOutput, calls=%fused_computation.12 | convolution fusion | flops 503316480 | bytes 3506176 | tf_op jit(solution)/shard_map/erd,efd->erf/dot_general | solution.py:104
  156.3 0.7 fusion.20
  157.0 9.8 %all_gather.27 = bf16[480,1024]{1,0:T(8,128)(2,1)S(1)} all-gather(bf16[480,256]{1,0:T(8,128)(2,1)S(1)} %fusion.20), channel_id=1, replica_groups=mesh['sp'=8,'tp'=4] {'tp'}, dimensions={1}, use_global_device_ids=true | all-gather | bytes 1228800 | tf_op jit(solution)/shard_map/all_gather | solution.py:110
  166.8 0.7 fusion.15
  167.5 0.8 copy.95
  168.9 3.7 %reduce.4 = bf16[480,512]{1,0:T(8,128)(2,1)S(1)} reduce(bf16[480,1,512]{2,1,0:T(2,128)(2,1)S(1)} %bitcast.81, bf16[]{:T(256)} %broadcast.119), dimensions={1}, to_apply=%bitcast.78.reduce_sub_computation | reduce | bytes 983042
  172.5 1.0 reshape.198
  173.5 5.5 %all-to-all-start.1 = ((bf16[8,2,15360]{2,1,0:T(2,128)(2,1)}), bf16[8,2,15360]{2,1,0:T(2,128)(2,1)S(1)}, u32[]{:S(2)}, u32[]{:S(2)}) async-start(bf16[8,2,15360]{2,1,0:T(2,128)(2,1)} %reshape.198), calls=%async_computation.1 | async-start | bytes 983040 | tf_op jit(solution)/shard_map/all_to_all | solution.py:118
  179.3 1.7 fusion.43
  181.1 1.7 fusion.25
  182.8 6.3 %all_gather.25 = bf16[192,1024]{1,0:T(8,128)(2,1)S(1)} all-gather(bf16[192,256]{1,0:T(8,128)(2,1)S(1)} %fusion.25), channel_id=1, replica_groups=mesh['sp'=8,'tp'=4] {'tp'}, dimensions={1}, use_global_device_ids=true | all-gather | bytes 491520 | tf_op jit(solution)/shard_map/all_gather | solution.py:109
  189.1 4.2 %all-to-all-done.1 = bf16[8,2,15360]{2,1,0:T(2,128)(2,1)S(1)} async-done(((bf16[8,2,15360]{2,1,0:T(2,128)(2,1)}), bf16[8,2,15360]{2,1,0:T(2,128)(2,1)S(1)}, u32[]{:S(2)}, u32[]{:S(2)}) %all-to-all-start.1) | async-done | bytes 491552 | tf_op jit(solution)/shard_map/all_to_all | solution.py:118
  193.9 2.1 gather_fusion.1
  196.1 1.6 multiply_reduce_fusion
  197.7 2.0 fusion.24
  (67 shorter events, 4.8 us)
Async XLA Ops:
  6.5 160.3 %copy-start = (bf16[1,1024,512]{2,1,0:T(8,128)(2,1)S(1)}, bf16[1,1024,512]{2,1,0:T(8,128)(2,1)}, u32[]{:S(2)}) copy-start(bf16[1,1024,512]{2,1,0:T(8,128)(2,1)} %param.28) | copy-start | bytes 3145732
  6.5 147.0 %all-gather.2.cloned.1.call-start = ((), (), s32[]{:S(2)}) async-start(), calls=%async_computation.2 | async-start | bytes 2457600 | tf_op jit(solution)/shard_map/all_gather | solution.py:103
  50.5 4.5 %copy-start.2 = (bf16[192,256]{1,0:T(8,128)(2,1)S(1)}, bf16[192,256]{1,0:T(8,128)(2,1)}, u32[]{:S(2)}) copy-start(bf16[192,256]{1,0:T(8,128)(2,1)} %param.19) | copy-start | bytes 294916
  87.4 4.1 %copy-start.5 = (f32[4]{0:T(128)S(1)}, f32[4]{0:T(128)}, u32[]{:S(2)}) copy-start(f32[4]{0:T(128)} %param.20) | copy-start | bytes 52
  87.4 4.2 %copy-start.7 = (f32[64]{0:T(128)S(1)}, f32[64]{0:T(128)}, u32[]{:S(2)}) copy-start(f32[64]{0:T(128)} %param.21) | copy-start | bytes 772
  87.4 11.6 %copy-start.9 = (bf16[1024,512]{1,0:T(8,128)(2,1)S(1)}, bf16[1024,512]{1,0:T(8,128)(2,1)}, u32[]{:S(2)}) copy-start(bf16[1024,512]{1,0:T(8,128)(2,1)} %param.22) | copy-start | bytes 3145732
  87.4 11.5 %copy-start.11 = (bf16[192,512]{1,0:T(8,128)(2,1)S(1)}, bf16[192,512]{1,0:T(8,128)(2,1)}, u32[]{:S(2)}) copy-start(bf16[192,512]{1,0:T(8,128)(2,1)} %param.16) | copy-start | bytes 589828
  91.4 17.7 %copy-start.4 = (f32[2048]{0:T(1024)S(1)}, f32[2048]{0:T(1024)}, u32[]{:S(2)}) copy-start(f32[2048]{0:T(1024)} %param.23) | copy-start | bytes 24580
  133.3 22.9 %copy-start.10 = (bf16[1,256,2048]{2,1,0:T(8,128)(2,1)S(1)}, bf16[1,256,2048]{2,1,0:T(8,128)(2,1)}, u32[]{:S(2)}) copy-start(bf16[1,256,2048]{2,1,0:T(8,128)(2,1)} %param.27) | copy-start | bytes 3145732
  153.6 2.7 %copy-start.8 = (bf16[1,480,2048]{2,1,0:T(8,128)(2,1)S(1)}, bf16[1,480,2048]{2,1,0:T(8,128)(2,1)}, u32[]{:S(2)}) copy-start(bf16[1,480,2048]{2,1,0:T(8,128)(2,1)} %all-gather.2.cloned.1.call-done) | copy-start | bytes 5898244
  157.0 22.0 %copy-start.3 = (s32[192,2]{0,1:T(2,128)S(1)}, s32[192,2]{0,1:T(2,128)}, u32[]{:S(2)}) copy-start(s32[192,2]{0,1:T(2,128)} %param.24) | copy-start | bytes 4612
  157.0 22.2 %copy-start.6 = (f32[192,2]{0,1:T(2,128)S(1)}, f32[192,2]{0,1:T(2,128)}, u32[]{:S(2)}) copy-start(f32[192,2]{0,1:T(2,128)} %param.25) | copy-start | bytes 4612
  173.5 19.8 %all-to-all-start.1 = ((bf16[8,2,15360]{2,1,0:T(2,128)(2,1)}), bf16[8,2,15360]{2,1,0:T(2,128)(2,1)S(1)}, u32[]{:S(2)}, u32[]{:S(2)}) async-start(bf16[8,2,15360]{2,1,0:T(2,128)(2,1)} %reshape.198), calls=%async_computation.1 | async-start | bytes 983040 | tf_op jit(solution)/shard_map/all_to_all | solution.py:118
  193.9 3.9 %copy-start.1 = (bf16[1024,512]{1,0:T(8,128)(2,1)S(1)}, bf16[1024,512]{1,0:T(8,128)(2,1)}, u32[]{:S(2)}) copy-start(bf16[1024,512]{1,0:T(8,128)(2,1)} %param.31) | copy-start | bytes 3145732
Sparse Core Ops, SparseCore 0:
  133.3 20.2 all-gather.1
where the time goes:
time: 207 us
  blocking collectives  119 us (57%)
  waiting for transfers between devices  24.4 us (12%)
  matrix products  16.5 us (8%)
  local copies, waits for them, and re-layouts  15.1 us (7%)
  between operations  13.8 us (7%)
  other arithmetic  12.6 us (6%)
  starting transfers between devices  5.51 us (3%)
    all_gather x1, blocking collectives, body(): key_piece = lax.all_gather(key_rows, 'sp', axis=0, tiled=True)  34.1 us
    all_gather x1, blocking collectives, body(): value_piece = lax.all_gather(value_rows, 'sp', axis=0, tiled=True)  32.1 us
    all_to_all x1, blocking collectives, body(): lax.all_to_all(outgoing, 'sp', split_axis=0, concat_axis=1, tiled=True)  20.3 us
    all_gather x1, waiting for transfers between devices, body(): pieces = lax.all_gather(arrived, 'tp', axis=2, tiled=True)  20.1 us
    all_gather x1, blocking collectives, body(): lax.all_gather(expert_flat, 'tp', axis=1, tiled=True)  9.84 us
    all_gather x1, blocking collectives, body(): full_rows = lax.all_gather(hidden_state, 'tp', axis=1, tiled=True)  8.9 us
    all_gather x1, blocking collectives, body(): lax.all_gather(head_out, 'tp', axis=1, tiled=True)  7.21 us
    all_gather x1, blocking collectives, body(): lax.all_gather(shared_hidden, 'tp', axis=1, tiled=True)  6.29 us
  transfers between devices with their start and end apart: 2, of which 2 were waited for; matrix products, arithmetic and copies ran while one was open for 2% of the time, Pallas kernels for 0%

commit v1 on v0

--- a/solution.py
+++ b/solution.py
@@ -5,6 +5,16 @@
 
 epsilon = 1e-06
 masked_score = -1e30
+
+
+def pass_along(x, axis, along):
+    size = lax.axis_size(axis)
+    moving, blocks = (x, [x])
+    for _ in range(size - 1):
+        moving = lax.ppermute(moving, axis, [(i, (i + 1) % size) for i in range(size)])
+        blocks.insert(0, moving)
+    merged = jnp.concatenate(blocks, axis=along)
+    return jnp.roll(merged, (lax.axis_index(axis) + 1) * x.shape[along], axis=along)
 
 
 def rms_scale(values, gain_vec):
@@ -100,7 +110,7 @@
     outgoing = jnp.take(padded, slot_token, axis=0).reshape(experts_all, capacity, col_dev)
     arrived = lax.all_to_all(outgoing, "sp", split_axis=0, concat_axis=1, tiled=True)
     arrived_rows = arrived.shape[1]
-    pieces = lax.all_gather(arrived, "tp", axis=2, tiled=True)
+    pieces = pass_along(arrived, "tp", 2)
     gate_add = jnp.einsum("erd,efd->erf", pieces, expert_gate, preferred_element_type=jnp.float32)
     up_add = jnp.einsum("erd,efd->erf", pieces, expert_up, preferred_element_type=jnp.float32)
     expert_hidden = (jax.nn.silu(gate_add) * up_add).astype(jnp.bfloat16)

time: 207 us -> 196 us (0.947)
  between operations: 13.8 us -> 0.49 us
  waiting for transfers between devices: 24.4 us -> 28.7 us
    ppermute x0 -> x3, waiting for transfers between devices: none -> 24.6 us  [pass_along(): lax.ppermute(moving, axis, [(i, (i + 1) % size) for i in range(size)])]
    all_gather x1 -> x0, waiting for transfers between devices: 20.1 us -> none  [body(): pieces = lax.all_gather(arrived, 'tp', axis=2, tiled=True)]
    unnamed x31 -> x38, local copies, waits for them, and re-layouts: 4.14 us -> 6.92 us
  transfers between devices with their start and end apart: 2 -> 4, of which waited for: 2 -> 4; matrix products, arithmetic and copies ran while one was open for 2% -> 2% of each run, Pallas kernels for 0% -> 0%
where the time goes in v1:
time: 196 us; the launch traced here: 195 us
  blocking collectives  118 us (60%)
  waiting for transfers between devices  28.7 us (15%)
  local copies, waits for them, and re-layouts  17.1 us (9%)
  matrix products  14.5 us (7%)
  other arithmetic  12.6 us (6%)
  starting transfers between devices  3.7 us (2%)
    all_gather x1, blocking collectives, body(): key_piece = lax.all_gather(key_rows, 'sp', axis=0, tiled=True)  34.1 us
    all_gather x1, blocking collectives, body(): value_piece = lax.all_gather(value_rows, 'sp', axis=0, tiled=True)  32.1 us
    ppermute x3, waiting for transfers between devices, pass_along(): lax.ppermute(moving, axis, [(i, (i + 1) % size) for i in range(size)])  24.6 us
    all_to_all x1, blocking collectives, body(): lax.all_to_all(outgoing, 'sp', split_axis=0, concat_axis=1, tiled=True)  20.3 us
    all_gather x1, blocking collectives, body(): lax.all_gather(expert_flat, 'tp', axis=1, tiled=True)  8.99 us
    all_gather x1, blocking collectives, body(): full_rows = lax.all_gather(hidden_state, 'tp', axis=1, tiled=True)  8.91 us
    all_gather x1, blocking collectives, body(): lax.all_gather(head_out, 'tp', axis=1, tiled=True)  7.19 us
    unnamed x38, local copies, waits for them, and re-layouts  6.92 us
  transfers between devices with their start and end apart: 4, of which 4 were waited for; matrix products, arithmetic and copies ran while one was open for 2% of the time, Pallas kernels for 0%

profile of v1, /device:TPU:0, one launch (start us, length us, event | category | flops | bytes accessed | tf_op | source)
XLA Modules:
  0.0 195.2 jit_solution(17674878508784875244)
XLA Ops:
  0.0 0.9 copy.68
  1.9 0.8 reduce-window.6
  3.5 2.9 %scatter_custom_fusion = s32[480]{0:T(512)S(1)} fusion(s32[384]{0:T(512)S(1)} %fusion.36, s32[384]{0:T(512)S(1)} %reshape.188, s32[]{:T(128)} %constant.51.clone.1), kind=kCustom, calls=%fused_computation.75 | custom fusion | bytes 1924 | tf_op jit(solution)/shard_map/scatter | solution.py:106
  6.7 34.1 %all_gather.18 = bf16[1536,256]{1,0:T(8,128)(2,1)S(1)} all-gather(bf16[192,256]{1,0:T(8,128)(2,1)} %param.18), channel_id=1, replica_groups=mesh['sp'=8,'tp'=4] {'sp'}, dimensions={0}, use_global_device_ids=true | all-gather | bytes 884736 | tf_op jit(solution)/shard_map/all_gather | solution.py:65
  41.1 1.0 copy.60
  42.1 1.9 fusion
  44.0 4.4 %fusion.1 = (f32[2,4,192]{2,1,0:T(4,128)S(1)}, bf16[2,4,192,1536]{3,2,1,0:T(8,128)(2,1)}) fusion(f32[2,4,192,1536]{3,2,1,0:T(8,128)S(1)} %get-tuple-element.8, f32[2,4,192]{2,1,0:T(4,128)S(1)} %broadcast_maximum_fusion, pred[192,1536]{1,0:T(8,128)(4,1)S(1)} %iota_compare_fusion), kind=kLoop, calls=%fused_computation.6 | loop fusion | flops 14154240 | bytes 14462976 | tf_op jit(solution)/shard_map/reduce_sum | solution.py:80
  48.4 32.1 %all_gather.19 = bf16[1536,256]{1,0:T(8,128)(2,1)S(1)} all-gather(bf16[192,256]{1,0:T(8,128)(2,1)S(1)} %copy-done.2), channel_id=1, replica_groups=mesh['sp'=8,'tp'=4] {'sp'}, dimensions={0}, use_global_device_ids=true | all-gather | bytes 884736 | tf_op jit(solution)/shard_map/all_gather | solution.py:66
  80.9 4.0 %fusion.25 = f32[2,4,192,64]{2,3,0,1:T(8,128)S(1)} fusion(bf16[1536,4,64,1]{0,2,3,1:T(8,128)(2,1)S(1)} %bitcast.84, bf16[2,4,192,1536]{3,2,1,0:T(8,128)(2,1)} %get-tuple-element.6, f32[2,4,192]{2,0,1:T(2,128)S(1)} %copy.66), kind=kOutput, calls=%fused_computation.35 | convolution fusion | flops 302088192 | bytes 5904384 | tf_op jit(solution)/shard_map/mhqk,khd->mhqd/dot_general | solution.py:81
  85.2 7.2 %all_gather.20 = bf16[192,1024]{0,1:T(8,128)(2,1)S(1)} all-gather(bf16[192,256]{0,1:T(8,128)(2,1)S(1)} %bitcast.85), channel_id=1, replica_groups=mesh['sp'=8,'tp'=4] {'tp'}, dimensions={1}, use_global_device_ids=true | all-gather | bytes 491520 | tf_op jit(solution)/shard_map/all_gather | solution.py:89
  92.4 1.1 fusion.19
  93.5 8.9 %all_gather.21 = bf16[192,2048]{1,0:T(8,128)(2,1)S(1)} all-gather(bf16[192,512]{1,0:T(8,128)(2,1)} %fusion.19), channel_id=1, replica_groups=mesh['sp'=8,'tp'=4] {'tp'}, dimensions={1}, use_global_device_ids=true | all-gather | bytes 983040 | tf_op jit(solution)/shard_map/all_gather | solution.py:94
  103.0 2.1 %gather_fusion = bf16[480,512]{1,0:T(8,128)(2,1)S(1)} fusion(bf16[193,512]{1,0:T(8,128)(2,1)S(1)} %concatenate.9, s32[1024]{0:T(1024)S(1)} %get-tuple-element.10), kind=kCustom, calls=%fused_computation | custom fusion | bytes 984960 | tf_op jit(solution)/shard_map/jit(_take)/gather | solution.py:110
  105.4 20.3 %all_to_all.21 = bf16[8,60,512]{2,1,0:T(8,128)(2,1)S(1)} all-to-all(bf16[8,60,512]{2,1,0:T(8,128)(2,1)S(1)} %broadcast_select_fusion.1), channel_id=1, replica_groups=mesh['sp'=8,'tp'=4] {'sp'}, dimensions={0} | all-to-all | bytes 983040 | tf_op jit(solution)/shard_map/all_to_all | solution.py:111
  125.9 8.2 %collective-permute-done = bf16[1,480,512]{2,1,0:T(8,128)(2,1)S(1)} collective-permute-done((bf16[1,480,512]{2,1,0:T(8,128)(2,1)S(1)}, bf16[1,480,512]{2,1,0:T(8,128)(2,1)S(1)}, u32[]{:S(2)}, u32[]{:S(2)}) %collective-permute-start) | collective-permute-done | bytes 491552 | tf_op jit(solution)/shard_map/ppermute | solution.py:14
  134.1 8.3 %collective-permute-done.1 = bf16[1,480,512]{2,1,0:T(8,128)(2,1)S(1)} collective-permute-done((bf16[1,480,512]{2,1,0:T(8,128)(2,1)S(1)}, bf16[1,480,512]{2,1,0:T(8,128)(2,1)S(1)}, u32[]{:S(2)}, u32[]{:S(2)}) %collective-permute-start.1) | collective-permute-done | bytes 491552 | tf_op jit(solution)/shard_map/ppermute | solution.py:14
  142.6 8.1 %collective-permute-done.2 = bf16[1,480,512]{2,1,0:T(8,128)(2,1)} collective-permute-done((bf16[1,480,512]{2,1,0:T(8,128)(2,1)S(1)}, bf16[1,480,512]{2,1,0:T(8,128)(2,1)}, u32[]{:S(2)}, u32[]{:S(2)}) %collective-permute-start.2) | collective-permute-done | bytes 491552 | tf_op jit(solution)/shard_map/ppermute | solution.py:14
  150.8 1.1 constant_dynamic-update-slice_fusion.7
  152.0 1.1 constant_dynamic-update-slice_fusion.3
  154.4 0.7 multiply_convert_fusion
  155.1 9.0 %all_gather.23 = bf16[480,1024]{1,0:T(8,128)(2,1)S(1)} all-gather(bf16[480,256]{1,0:T(8,128)(2,1)S(1)} %multiply_convert_fusion), channel_id=1, replica_groups=mesh['sp'=8,'tp'=4] {'tp'}, dimensions={1}, use_global_device_ids=true | all-gather | bytes 1228800 | tf_op jit(solution)/shard_map/all_gather | solution.py:120
  164.8 0.8 copy.95
  166.2 3.7 %reduce.4 = bf16[480,512]{1,0:T(8,128)(2,1)S(1)} reduce(bf16[480,1,512]{2,1,0:T(2,128)(2,1)S(1)} %bitcast.81, bf16[]{:T(256)} %broadcast.120), dimensions={1}, to_apply=%bitcast.78.reduce_sub_computation | reduce | bytes 983042
  169.8 1.0 reshape.198
  170.8 3.6 %all-to-all-start.1 = ((bf16[8,2,15360]{2,1,0:T(2,128)(2,1)}), bf16[8,2,15360]{2,1,0:T(2,128)(2,1)S(1)}, u32[]{:S(2)}, u32[]{:S(2)}) async-start(bf16[8,2,15360]{2,1,0:T(2,128)(2,1)} %reshape.198), calls=%async_computation.1 | async-start | bytes 983040 | tf_op jit(solution)/shard_map/all_to_all | solution.py:128
  174.8 1.7 fusion.45
  176.5 1.7 fusion.21
  178.2 6.4 %all_gather.22 = bf16[192,1024]{1,0:T(8,128)(2,1)S(1)} all-gather(bf16[192,256]{1,0:T(8,128)(2,1)S(1)} %fusion.21), channel_id=1, replica_groups=mesh['sp'=8,'tp'=4] {'tp'}, dimensions={1}, use_global_device_ids=true | all-gather | bytes 491520 | tf_op jit(solution)/shard_map/all_gather | solution.py:119
  184.7 4.1 %all-to-all-done.1 = bf16[8,2,15360]{2,1,0:T(2,128)(2,1)S(1)} async-done(((bf16[8,2,15360]{2,1,0:T(2,128)(2,1)}), bf16[8,2,15360]{2,1,0:T(2,128)(2,1)S(1)}, u32[]{:S(2)}, u32[]{:S(2)}) %all-to-all-start.1) | async-done | bytes 491552 | tf_op jit(solution)/shard_map/all_to_all | solution.py:128
  189.3 2.1 %gather_fusion.1 = bf16[384,512]{1,0:T(8,128)(2,1)S(1)} fusion(bf16[480,512]{1,0:T(8,128)(2,1)S(1)} %bitcast.80, s32[1024]{0:T(1024)S(1)} %get-tuple-element.9), kind=kCustom, calls=%fused_computation.1 | custom fusion | bytes 787968 | tf_op jit(solution)/shard_map/jit(_take)/gather | solution.py:133
  191.6 1.6 multiply_reduce_fusion
  193.2 2.0 %fusion.20 = bf16[192,512]{1,0:T(8,128)(2,1)} fusion(f32[192,512]{1,0:T(8,128)S(1)} %multiply_reduce_fusion, bf16[192,1024]{1,0:T(8,128)(2,1)S(1)} %all_gather.22, bf16[1024,512]{1,0:T(8,128)(2,1)S(1)} %copy-done.1, bf16[192,512]{1,0:T(8,128)(2,1)} %fusion.19), kind=kOutput, calls=%fused_computation.29 | convolution fusion | flops 201719808 | bytes 2228224 | tf_op jit(solution)/shard_map/dot_general | solution.py:124
  (77 shorter events, 7.7 us)
Async XLA Ops:
  0.0 164.1 %copy-start = (bf16[1,1024,512]{2,1,0:T(8,128)(2,1)S(1)}, bf16[1,1024,512]{2,1,0:T(8,128)(2,1)}, u32[]{:S(2)}) copy-start(bf16[1,1024,512]{2,1,0:T(8,128)(2,1)} %param.28) | copy-start | bytes 3145732
  44.0 4.5 %copy-start.2 = (bf16[192,256]{1,0:T(8,128)(2,1)S(1)}, bf16[192,256]{1,0:T(8,128)(2,1)}, u32[]{:S(2)}) copy-start(bf16[192,256]{1,0:T(8,128)(2,1)} %param.19) | copy-start | bytes 294916
  80.8 4.1 %copy-start.5 = (f32[4]{0:T(128)S(1)}, f32[4]{0:T(128)}, u32[]{:S(2)}) copy-start(f32[4]{0:T(128)} %param.20) | copy-start | bytes 52
  80.8 4.2 %copy-start.7 = (f32[64]{0:T(128)S(1)}, f32[64]{0:T(128)}, u32[]{:S(2)}) copy-start(f32[64]{0:T(128)} %param.21) | copy-start | bytes 772
  80.8 11.5 %copy-start.8 = (bf16[1024,512]{1,0:T(8,128)(2,1)S(1)}, bf16[1024,512]{1,0:T(8,128)(2,1)}, u32[]{:S(2)}) copy-start(bf16[1024,512]{1,0:T(8,128)(2,1)} %param.22) | copy-start | bytes 3145732
  80.9 11.5 %copy-start.11 = (bf16[192,512]{1,0:T(8,128)(2,1)S(1)}, bf16[192,512]{1,0:T(8,128)(2,1)}, u32[]{:S(2)}) copy-start(bf16[192,512]{1,0:T(8,128)(2,1)} %param.16) | copy-start | bytes 589828
  84.9 17.7 %copy-start.4 = (f32[2048]{0:T(1024)S(1)}, f32[2048]{0:T(1024)}, u32[]{:S(2)}) copy-start(f32[2048]{0:T(1024)} %param.23) | copy-start | bytes 24580
  125.8 8.3 %collective-permute-start = (bf16[1,480,512]{2,1,0:T(8,128)(2,1)S(1)}, bf16[1,480,512]{2,1,0:T(8,128)(2,1)S(1)}, u32[]{:S(2)}, u32[]{:S(2)}) collective-permute-start(bf16[1,480,512]{2,1,0:T(8,128)(2,1)S(1)} %all_to_all.7), channel_id=1, source_target_pairs={{0,1},{1,2},{2,3},{3,0},{4,5},{5,6},{6,7},{7,4},{8,9},{9,10},{10,1... | collective-permute-start | bytes 1474568 | tf_op jit(solution)/shard_map/ppermute | solution.py:14
  134.1 8.3 %collective-permute-start.1 = (bf16[1,480,512]{2,1,0:T(8,128)(2,1)S(1)}, bf16[1,480,512]{2,1,0:T(8,128)(2,1)S(1)}, u32[]{:S(2)}, u32[]{:S(2)}) collective-permute-start(bf16[1,480,512]{2,1,0:T(8,128)(2,1)S(1)} %collective-permute-done), channel_id=1, source_target_pairs={{0,1},{1,2},{2,3},{3,0},{4,5},{5,6},{6,7},{7,4},{8,9},{9,10},{10,1... | collective-permute-start | bytes 1474568 | tf_op jit(solution)/shard_map/ppermute | solution.py:14
  142.4 8.4 %collective-permute-start.2 = (bf16[1,480,512]{2,1,0:T(8,128)(2,1)S(1)}, bf16[1,480,512]{2,1,0:T(8,128)(2,1)}, u32[]{:S(2)}, u32[]{:S(2)}) collective-permute-start(bf16[1,480,512]{2,1,0:T(8,128)(2,1)S(1)} %collective-permute-done.1), channel_id=1, source_target_pairs={{0,1},{1,2},{2,3},{3,0},{4,5},{5,6},{6,7},{7,4},{8,9},{9,10},{10,1... | collective-permute-start | bytes 1474568 | tf_op jit(solution)/shard_map/ppermute | solution.py:14
  142.6 10.7 %copy-start.9 = (bf16[1,256,2048]{2,1,0:T(8,128)(2,1)S(1)}, bf16[1,256,2048]{2,1,0:T(8,128)(2,1)}, u32[]{:S(2)}) copy-start(bf16[1,256,2048]{2,1,0:T(8,128)(2,1)} %param.26) | copy-start | bytes 3145732
  153.2 1.2 copy-start.10
  164.1 10.3 %copy-start.3 = (s32[192,2]{0,1:T(2,128)S(1)}, s32[192,2]{0,1:T(2,128)}, u32[]{:S(2)}) copy-start(s32[192,2]{0,1:T(2,128)} %param.24) | copy-start | bytes 4612
  164.1 10.5 %copy-start.6 = (f32[192,2]{0,1:T(2,128)S(1)}, f32[192,2]{0,1:T(2,128)}, u32[]{:S(2)}) copy-start(f32[192,2]{0,1:T(2,128)} %param.25) | copy-start | bytes 4612
  170.8 18.0 %all-to-all-start.1 = ((bf16[8,2,15360]{2,1,0:T(2,128)(2,1)}), bf16[8,2,15360]{2,1,0:T(2,128)(2,1)S(1)}, u32[]{:S(2)}, u32[]{:S(2)}) async-start(bf16[8,2,15360]{2,1,0:T(2,128)(2,1)} %reshape.198), calls=%async_computation.1 | async-start | bytes 983040 | tf_op jit(solution)/shard_map/all_to_all | solution.py:128
  189.3 3.9 %copy-start.1 = (bf16[1024,512]{1,0:T(8,128)(2,1)S(1)}, bf16[1024,512]{1,0:T(8,128)(2,1)}, u32[]{:S(2)}) copy-start(bf16[1024,512]{1,0:T(8,128)(2,1)} %param.31) | copy-start | bytes 3145732
